TPU v7x, 32 devices: a whole 2x2x4 slice. The times are simulated.
32 devices in a mesh: sp: 16 (over z, y, x), tp: 2 (over core).
Axes of the slice: x: 2, y: 2, z: 4, core: 2. Of those that a mesh axis runs over, the one named last changes fastest.
Arguments:
- residual: bfloat16 [4096, 2048], P(('sp', 'tp')), may hold values from -6 to 6
- query_one: bfloat16 [4096, 512], P('sp', 'tp'), may hold values from -6.5 to 6.5
- key_one: bfloat16 [4096, 512], P('sp', 'tp'), may hold values from -6.5 to 6.5
- query_two: bfloat16 [4096, 512], P('sp', 'tp'), may hold values from -6.5 to 6.5
- key_two: bfloat16 [4096, 512], P('sp', 'tp'), may hold values from -6.5 to 6.5
- value_rows: bfloat16 [4096, 1024], P('sp', 'tp'), may hold values from -6 to 6
- lambda_head: float32 [8], P('tp'), may hold values from 0.3 to 0.8
- head_gain: float32 [128], replicated, may hold values from 0.1 to 1.9
- out_weight: bfloat16 [1024, 2048], replicated, may hold values from -0.1875 to 0.1875
- norm_gain: float32 [2048], replicated, may hold values from 0.1 to 1.9
- route_ids: int32 [4096, 2], P(('sp', 'tp')), may hold values from 0 to 15, all different within a row; in each aligned block of 128 rows (0 to 127, 128 to 255, ...) at most 24 rows name the same one
- route_weights: float32 [4096, 2], P(('sp', 'tp')), may hold values from 0.25 to 1
- gate_weight: bfloat16 [16, 2048, 512], P('sp', None, 'tp'), may hold values from -0.125 to 0.125
- up_weight: bfloat16 [16, 2048, 512], P('sp', None, 'tp'), may hold values from -0.125 to 0.125
- down_weight: bfloat16 [16, 512, 2048], P('sp', 'tp'), may hold values from -0.25 to 0.25
Outputs:
- mixed: bfloat16 [4096, 2048], P(('sp', 'tp'))
Inputs may be any that keep to these rules, and one draw needn't show every extreme that they name: `route_ids`: each row names 2 different experts. Among the rows of one device (aligned blocks of 128 rows) no expert is named more than 24 times, and in every draw some device has an expert named exactly 24 times.
All inputs are finite; a program needn't handle non-finite values.
Results may differ from a plain program's by a relative error of at most 0.014.
Values may be sent and summed in bfloat16 or wider, within the bound.
A program may use at most 128 MiB of HBM per device.

v0:
```python
import jax
import jax.numpy as jnp
from jax import lax
from jax.sharding import PartitionSpec as P

epsilon = 1e-06
low_value = -1e30


def online_update(carried, queries, keys_block, values_block, query_pos, key_pos, score_scale):
    running_max, running_sum, summed = carried
    scores = (
        jnp.einsum("qhd,khd->qhk", queries, keys_block, preferred_element_type=jnp.float32)
        * score_scale
    )
    allowed = (query_pos[:, None] >= key_pos[None, :])[:, None, :]
    scores = jnp.where(allowed, scores, low_value)
    newest = jnp.maximum(running_max, jnp.max(scores, axis=-1))
    exp_weights = jnp.where(allowed, jnp.exp(scores - newest[..., None]), 0.0)
    factor = jnp.exp(running_max - newest)
    running_sum = running_sum * factor + jnp.sum(exp_weights, axis=-1)
    product = jnp.einsum(
        "qhk,khd->qhd",
        exp_weights.astype(jnp.bfloat16),
        values_block,
        preferred_element_type=jnp.float32,
    )
    summed = summed * factor[..., None] + product
    return (newest, running_sum, summed)


def expert_rows(rows, gate_half, up_half, down_half):
    gate = jnp.dot(rows, gate_half, preferred_element_type=jnp.float32)
    upper = jnp.dot(rows, up_half, preferred_element_type=jnp.float32)
    hidden = (jax.nn.silu(gate) * upper).astype(jnp.bfloat16)
    return jnp.dot(hidden, down_half, preferred_element_type=jnp.float32)


def on_device(
    residual,
    query_one,
    key_one,
    query_two,
    key_two,
    value_rows,
    lambda_head,
    head_gain,
    out_weight,
    norm_gain,
    route_ids,
    route_weights,
    gate_weight,
    up_weight,
    down_weight,
):
    row_count = query_one.shape[0]
    head_count = lambda_head.shape[0]
    head_dim = query_one.shape[1] // head_count
    value_dim = value_rows.shape[1] // head_count
    model_width = residual.shape[1]
    sp_count = lax.axis_size("sp")
    score_scale = head_dim ** (-0.5)
    offset = lax.axis_index("sp") * row_count
    query_pos = offset + jnp.arange(row_count)
    last_query = offset + row_count - 1
    first_query = query_one.reshape(row_count, head_count, head_dim)
    second_query = query_two.reshape(row_count, head_count, head_dim)
    empty_state = (
        jnp.full((row_count, head_count), low_value, jnp.float32),
        jnp.zeros((row_count, head_count), jnp.float32),
        jnp.zeros((row_count, head_count, value_dim), jnp.float32),
    )
    pieces = (
        lax.all_gather(key_one, "sp", axis=0, tiled=True),
        lax.all_gather(key_two, "sp", axis=0, tiled=True),
        lax.all_gather(value_rows, "sp", axis=0, tiled=True),
    )
    piece_rows = pieces[0].shape[0]
    width_block = 512

    def one_block(position, inner_state):
        begin_row = position * width_block

        def advance(current):
            first_keys = lax.dynamic_slice_in_dim(pieces[0], begin_row, width_block, 0).reshape(
                width_block, head_count, head_dim
            )
            second_keys = lax.dynamic_slice_in_dim(pieces[1], begin_row, width_block, 0).reshape(
                width_block, head_count, head_dim
            )
            value_part = lax.dynamic_slice_in_dim(pieces[2], begin_row, width_block, 0).reshape(
                width_block, head_count, value_dim
            )
            key_pos = begin_row + jnp.arange(width_block)
            first_next = online_update(
                current[0], first_query, first_keys, value_part, query_pos, key_pos, score_scale
            )
            second_next = online_update(
                current[1], second_query, second_keys, value_part, query_pos, key_pos, score_scale
            )
            return (first_next, second_next)

        return lax.cond(begin_row <= last_query, advance, lambda unchanged: unchanged, inner_state)

    first_state, second_state = lax.fori_loop(
        0, piece_rows // width_block, one_block, (empty_state, empty_state)
    )
    first_out = first_state[2] / first_state[1][..., None]
    second_out = second_state[2] / second_state[1][..., None]
    head_out = first_out - lambda_head[None, :, None] * second_out
    normed = (
        head_out
        * lax.rsqrt(jnp.mean(head_out * head_out, axis=-1, keepdims=True) + epsilon)
        * head_gain
    )
    attended = normed.reshape(row_count, head_count * value_dim).astype(jnp.bfloat16)
    all_heads = lax.all_to_all(attended, "tp", split_axis=0, concat_axis=1, tiled=True)
    projected = jnp.dot(all_heads, out_weight, preferred_element_type=jnp.float32)
    after_float = (
        (residual.astype(jnp.float32) + projected).astype(jnp.bfloat16).astype(jnp.float32)
    )
    routed = (
        after_float
        * lax.rsqrt(jnp.mean(after_float * after_float, axis=-1, keepdims=True) + epsilon)
        * norm_gain
    ).astype(jnp.bfloat16)
    local_rows, top_count = route_ids.shape
    expert_count = gate_weight.shape[0] * sp_count
    capacity = max(2, (3 * row_count + 2 * sp_count - 1) // (2 * sp_count))
    flat_ids = route_ids.reshape(-1)
    onehot = (flat_ids[:, None] == jnp.arange(expert_count)[None, :]).astype(jnp.int32)
    rank = jnp.sum((jnp.cumsum(onehot, axis=0) - onehot) * onehot, axis=1)
    slot = flat_ids * capacity + rank
    source_row = jnp.arange(local_rows * top_count) // top_count
    slot_rows = jnp.full((expert_count * capacity,), -1, jnp.int32).at[slot].set(source_row)
    filled = (slot_rows >= 0)[:, None]
    outgoing = jnp.where(filled, routed[jnp.maximum(slot_rows, 0)], jnp.zeros((), jnp.bfloat16))
    outgoing = outgoing.reshape(expert_count, capacity, model_width)
    gate_half = gate_weight[0]
    up_half = up_weight[0]
    down_half = down_weight[0]
    both_halves = lax.all_gather(
        lax.all_to_all(outgoing, "sp", split_axis=0, concat_axis=0, tiled=True),
        "tp",
        axis=0,
        tiled=True,
    )
    sources, items, width_rows = both_halves.shape
    partial_value = expert_rows(
        both_halves.reshape(sources * items, width_rows), gate_half, up_half, down_half
    )
    partial_value = partial_value.reshape(sources, items, width_rows)
    summed = lax.psum_scatter(
        partial_value.astype(jnp.bfloat16), "tp", scatter_dimension=0, tiled=True
    )
    returned = lax.all_to_all(summed, "sp", split_axis=0, concat_axis=0, tiled=True)
    flat_back = returned.reshape(expert_count * capacity, model_width)
    picked = flat_back[slot].astype(jnp.float32).reshape(local_rows, top_count, model_width)
    moe_out = jnp.sum(picked * route_weights[..., None], axis=1)
    return (after_float + moe_out).astype(jnp.bfloat16)


def solution(mesh):
    placed = (
        P(("sp", "tp"), None),
        P("sp", "tp"),
        P("sp", "tp"),
        P("sp", "tp"),
        P("sp", "tp"),
        P("sp", "tp"),
        P("tp"),
        P(),
        P(),
        P(),
        P(("sp", "tp"), None),
        P(("sp", "tp"), None),
        P("sp", None, "tp"),
        P("sp", None, "tp"),
        P("sp", "tp", None),
    )
    return jax.shard_map(
        on_device, mesh=mesh, in_specs=placed, out_specs=P(("sp", "tp"), None), check_vma=False
    )
```

profile of v0, /device:TPU:12, one launch (start us, length us, event | category | flops | bytes accessed | tf_op | source)
XLA Modules:
  0.0 430.1 jit_solution(4854615677501949277)
XLA Ops:
  6.5 1.8 copy.52
  8.4 1.7 copy.55
  10.1 1.8 copy.54
  12.0 0.8 copy.60
  13.1 1.0 copy.53
  14.2 0.6 reduce-window.6
  15.4 1.4 scatter_custom_fusion
  17.0 57.3 %all-gather.5.cloned.1.call-done = bf16[4096,256]{0,1:T(8,128)(2,1)} async-done(((bf16[256,256]{0,1:T(8,128)(2,1)}), bf16[4096,256]{0,1:T(8,128)(2,1)}) %all-gather.5.cloned.1.call-update) | async-done | bytes 2097168 | tf_op jit(solution)/shard_map/all_gather | solution.py:74
  74.3 65.9 %all-gather.9.cloned.1.call-done = bf16[4096,256]{0,1:T(8,128)(2,1)} async-done(((bf16[256,256]{0,1:T(8,128)(2,1)}), bf16[4096,256]{0,1:T(8,128)(2,1)}) %all-gather.9.cloned.1.call-update) | async-done | bytes 2097168 | tf_op jit(solution)/shard_map/all_gather | solution.py:75
  140.1 86.9 %all-gather.7.cloned.1.call-done = bf16[4096,512]{0,1:T(8,128)(2,1)} async-done(((bf16[256,512]{0,1:T(8,128)(2,1)}), bf16[4096,512]{0,1:T(8,128)(2,1)}) %all-gather.7.cloned.1.call-update) | async-done | bytes 4194320 | tf_op jit(solution)/shard_map/all_gather | solution.py:76
  227.1 28.7 %while.24 = (s32[]{:T(128)}, f32[256,4]{0,1:T(4,128)S(1)}, f32[256,4]{0,1:T(4,128)S(1)}, f32[256,4,128]{0,2,1:T(8,128)S(1)}, f32[256,4]{0,1:T(4,128)S(1)}, /*ind...) while((s32[]{:T(128)}, f32[256,4]{0,1:T(4,128)S(1)}, ...), condition=%wide.region_7.8_spmd.clone, body=%wide.region_0.7_spmd.clone.sunk | while | flops 416944896 | bytes 21504444 | solution.py:105
  227.2 7.1 %conditional.3 = ((f32[256,4]{0,1:T(4,128)S(1)}, f32[256,4]{0,1:T(4,128)S(1)}, f32[256,4,128]{0,2,1:T(8,128)S(1)}, f32[256,4]{0,1:T(4,128)S(1)}, f32[256,4]{0,1:T(4,128)S(1)}, /*index=5*/f32[256,4,128]{0,2,1:T(8,128)S(1)})) conditional(s32[]{:T(128)} %convert_element_type.87, (f32[256,4]{0,1:T(4,128)S(1)}, f32[256,4]{0,1:T(4,128)S(1)}, ...), branch_computations={%region_1.0_spmd, %region_2.6_spmd} | conditional | flops 416944896 | bytes 21503086 | solution.py:103
  227.2 1.0 constant_dynamic-slice_fusion.2
  228.2 0.5 fusion.39
  228.7 1.0 constant_dynamic-slice_fusion
  229.8 0.7 fusion.3
  230.6 1.0 fusion.7
  231.7 1.1 constant_dynamic-slice_fusion.1
  232.7 0.8 fusion.8
  233.5 0.7 fusion.9
  234.3 7.1 %conditional.3 = ((f32[256,4]{0,1:T(4,128)S(1)}, f32[256,4]{0,1:T(4,128)S(1)}, f32[256,4,128]{0,2,1:T(8,128)S(1)}, f32[256,4]{0,1:T(4,128)S(1)}, f32[256,4]{0,1:T(4,128)S(1)}, /*index=5*/f32[256,4,128]{0,2,1:T(8,128)S(1)})) conditional(s32[]{:T(128)} %convert_element_type.87, (f32[256,4]{0,1:T(4,128)S(1)}, f32[256,4]{0,1:T(4,128)S(1)}, ...), branch_computations={%region_1.0_spmd, %region_2.6_spmd} | conditional | flops 416944896 | bytes 21503086 | solution.py:103
  234.3 1.0 constant_dynamic-slice_fusion.2
  235.3 0.5 fusion.39
  235.8 1.0 constant_dynamic-slice_fusion
  237.0 0.7 fusion.3
  237.7 1.0 fusion.7
  238.8 1.1 constant_dynamic-slice_fusion.1
  239.9 0.8 fusion.8
  240.6 0.7 fusion.9
  241.4 7.1 %conditional.3 = ((f32[256,4]{0,1:T(4,128)S(1)}, f32[256,4]{0,1:T(4,128)S(1)}, f32[256,4,128]{0,2,1:T(8,128)S(1)}, f32[256,4]{0,1:T(4,128)S(1)}, f32[256,4]{0,1:T(4,128)S(1)}, /*index=5*/f32[256,4,128]{0,2,1:T(8,128)S(1)})) conditional(s32[]{:T(128)} %convert_element_type.87, (f32[256,4]{0,1:T(4,128)S(1)}, f32[256,4]{0,1:T(4,128)S(1)}, ...), branch_computations={%region_1.0_spmd, %region_2.6_spmd} | conditional | flops 416944896 | bytes 21503086 | solution.py:103
  241.5 1.0 constant_dynamic-slice_fusion.2
  242.4 0.5 fusion.39
  242.9 1.0 constant_dynamic-slice_fusion
  244.1 0.7 fusion.3
  244.8 1.0 fusion.7
  245.9 1.1 constant_dynamic-slice_fusion.1
  247.0 0.8 fusion.8
  247.7 0.7 fusion.9
  248.6 7.1 %conditional.3 = ((f32[256,4]{0,1:T(4,128)S(1)}, f32[256,4]{0,1:T(4,128)S(1)}, f32[256,4,128]{0,2,1:T(8,128)S(1)}, f32[256,4]{0,1:T(4,128)S(1)}, f32[256,4]{0,1:T(4,128)S(1)}, /*index=5*/f32[256,4,128]{0,2,1:T(8,128)S(1)})) conditional(s32[]{:T(128)} %convert_element_type.87, (f32[256,4]{0,1:T(4,128)S(1)}, f32[256,4]{0,1:T(4,128)S(1)}, ...), branch_computations={%region_1.0_spmd, %region_2.6_spmd} | conditional | flops 416944896 | bytes 21503086 | solution.py:103
  248.6 1.0 constant_dynamic-slice_fusion.2
  249.6 0.5 fusion.39
  250.0 1.0 constant_dynamic-slice_fusion
  251.2 0.7 fusion.3
  252.0 1.0 fusion.7
  253.0 1.1 constant_dynamic-slice_fusion.1
  254.1 0.8 fusion.8
  254.9 0.7 fusion.9
  256.5 3.9 all_to_all.26
  260.6 3.0 multiply_reduce_fusion.1
  263.7 1.0 copy-done.1
  264.9 2.5 gather_fusion
  267.5 71.9 %all_to_all.27 = bf16[16,24,2048]{2,1,0:T(8,128)(2,1)} all-to-all(bf16[16,24,2048]{2,1,0:T(8,128)(2,1)S(1)} %broadcast_select_fusion), channel_id=1, replica_groups=mesh['sp'=16,'tp'=2] {'sp'}, dimensions={0} | all-to-all | bytes 3145728 | tf_op jit(solution)/shard_map/all_to_all | solution.py:143
  339.4 0.2 reduce-scatter.2.cloned.1.call-start
  339.6 11.4 %all-gather.11.cloned.1.call-done = bf16[32,24,2048]{2,1,0:T(8,128)(2,1)} async-done(((bf16[16,24,2048]{2,1,0:T(8,128)(2,1)}), bf16[32,24,2048]{2,1,0:T(8,128)(2,1)}) %all-gather.11.cloned.1.call-update) | async-done | bytes 3145744 | tf_op jit(solution)/shard_map/all_gather | solution.py:142
  351.0 3.0 fusion.31
  354.1 1.0 fusion.28
  355.1 2.6 convolution_convert_fusion
  357.8 12.6 %reduce-scatter.2.cloned.1.call-done = bf16[16,24,2048]{2,1,0:T(8,128)(2,1)} async-done(((bf16[32,24,2048]{2,1,0:T(8,128)(2,1)}), bf16[16,24,2048]{2,1,0:T(8,128)(2,1)}) %reduce-scatter.2.cloned.1.call-update) | async-done | bytes 1572880 | tf_op jit(solution)/shard_map/reduce_scatter | solution.py:153
  370.4 7.0 %all-to-all-start.2 = ((bf16[16,24,2048]{2,1,0:T(8,128)(2,1)}), bf16[16,24,2048]{2,1,0:T(8,128)(2,1)S(1)}, u32[]{:S(2)}, u32[]{:S(2)}) async-start(bf16[16,24,2048]{2,1,0:T(8,128)(2,1)} %reduce-scatter.2.cloned.1.call-done), calls=%async_computation.3 | async-start | bytes 3145728 | tf_op jit(solution)/shard_map/all_to_all | solution.py:156
  377.5 37.2 %all-to-all-done.2 = bf16[16,24,2048]{2,1,0:T(8,128)(2,1)S(1)} async-done(((bf16[16,24,2048]{2,1,0:T(8,128)(2,1)}), bf16[16,24,2048]{2,1,0:T(8,128)(2,1)S(1)}, u32[]{:S(2)}, u32[]{:S(2)}) %all-to-all-start.2) | async-done | bytes 1572896 | tf_op jit(solution)/shard_map/all_to_all | solution.py:156
  414.7 2.3 gather_fusion.1
  417.0 2.4 reshape.145
  419.4 3.2 multiply_reduce_fusion
  422.6 0.9 add_convert_fusion
  (112 shorter events, 3.5 us)
Async XLA Ops:
  6.5 348.6 %copy-start = (bf16[1,256,2048]{2,1,0:T(8,128)(2,1)S(1)}, bf16[1,256,2048]{2,1,0:T(8,128)(2,1)}, u32[]{:S(2)}) copy-start(bf16[1,256,2048]{2,1,0:T(8,128)(2,1)} %param.33) | copy-start | bytes 3145732
  6.5 8.5 %copy-start.6 = (s32[128,2]{0,1:T(2,128)S(1)}, s32[128,2]{0,1:T(2,128)}, u32[]{:S(2)}) copy-start(s32[128,2]{0,1:T(2,128)} %param.29) | copy-start | bytes 3076
  6.5 7.6 %copy-start.4 = (bf16[256,256]{1,0:T(8,128)(2,1)S(1)}, bf16[256,256]{1,0:T(8,128)(2,1)}, u32[]{:S(2)}) copy-start(bf16[256,256]{1,0:T(8,128)(2,1)} %param.22) | copy-start | bytes 393220
  6.5 67.7 %all-gather.5.cloned.1.call-start = ((), (), s32[]{:S(2)}) async-start(), calls=%async_computation.4 | async-start | bytes 2228224 | tf_op jit(solution)/shard_map/all_gather | solution.py:74
  8.4 131.8 %all-gather.9.cloned.1.call-start = ((), (), s32[]{:S(2)}) async-start(), calls=%async_computation.6 | async-start | bytes 2228224 | tf_op jit(solution)/shard_map/all_gather | solution.py:75
  10.1 216.9 %all-gather.7.cloned.1.call-start = ((), (), s32[]{:S(2)}) async-start(), calls=%async_computation.5 | async-start | bytes 4456448 | tf_op jit(solution)/shard_map/all_gather | solution.py:76
  12.0 339.0 %all-gather.11.cloned.1.call-start = ((), (), s32[]{:S(2)}) async-start(), calls=%async_computation.7 | async-start | bytes 4718592 | tf_op jit(solution)/shard_map/all_gather | solution.py:142
  227.1 28.8 %copy-start.8 = (f32[4]{0:T(128)S(1)}, f32[4]{0:T(128)}, u32[]{:S(2)}) copy-start(f32[4]{0:T(128)} %param.25) | copy-start | bytes 52
  227.1 29.0 %copy-start.9 = (f32[128]{0:T(128)S(1)}, f32[128]{0:T(128)}, u32[]{:S(2)}) copy-start(f32[128]{0:T(128)} %param.26) | copy-start | bytes 1540
  255.9 4.7 %copy-start.3 = (bf16[128,2048]{1,0:T(8,128)(2,1)S(1)}, bf16[128,2048]{1,0:T(8,128)(2,1)}, u32[]{:S(2)}) copy-start(bf16[128,2048]{1,0:T(8,128)(2,1)} %param.19) | copy-start | bytes 1572868
  260.6 4.1 copy-start.5
  263.7 1.0 copy-start.1
  267.5 83.5 %copy-start.11 = (bf16[1,2048,256]{2,1,0:T(8,128)(2,1)S(1)}, bf16[1,2048,256]{2,1,0:T(8,128)(2,1)}, u32[]{:S(2)}) copy-start(bf16[1,2048,256]{2,1,0:T(8,128)(2,1)} %param.31) | copy-start | bytes 3145732
  339.4 31.0 %reduce-scatter.2.cloned.1.call-start = ((), (), s32[]{:S(2)}) async-start(), calls=%async_computation.8 | async-start | bytes 4718592 | tf_op jit(solution)/shard_map/reduce_scatter | solution.py:153
  351.0 3.0 copy-start.10
  351.0 3.1 copy-start.12
  357.8 19.6 %copy-start.7 = (f32[128,2]{0,1:T(2,128)S(1)}, f32[128,2]{0,1:T(2,128)}, u32[]{:S(2)}) copy-start(f32[128,2]{0,1:T(2,128)} %param.30) | copy-start | bytes 3076
  370.4 44.3 %all-to-all-start.2 = ((bf16[16,24,2048]{2,1,0:T(8,128)(2,1)}), bf16[16,24,2048]{2,1,0:T(8,128)(2,1)S(1)}, u32[]{:S(2)}, u32[]{:S(2)}) async-start(bf16[16,24,2048]{2,1,0:T(8,128)(2,1)} %reduce-scatter.2.cloned.1.call-done), calls=%async_computation.3 | async-start | bytes 3145728 | tf_op jit(solution)/shard_map/all_to_all | solution.py:156
  419.4 3.2 copy-start.2
Sparse Core Ops, SparseCore 0:
  10.1 64.1 all-gather.4
  77.0 63.1 all-gather.8
  142.9 84.0 all-gather.6
  339.5 11.4 all-gather.10
  357.9 12.4 reduce-scatter.1
where the time goes:
time: 431 us; the launch traced here: 430 us
  waiting for transfers between devices  271 us (63%)
  blocking collectives  75.8 us (18%)
  local copies, waits for them, and re-layouts  30.4 us (7%)
  matrix products  20.6 us (5%)
  between operations  13.5 us (3%)
  other arithmetic  10.3 us (2%)
  starting transfers between devices  7.31 us (2%)
    all_gather x1, waiting for transfers between devices, on_device(): lax.all_gather(value_rows, 'sp', axis=0, tiled=True)  86.9 us
    all_to_all x1, blocking collectives, on_device(): lax.all_to_all(outgoing, 'sp', split_axis=0, concat_axis=0, tiled=True)  71.9 us
    all_gather x1, waiting for transfers between devices, on_device(): lax.all_gather(key_two, 'sp', axis=0, tiled=True)  65.9 us
    all_gather x1, waiting for transfers between devices, on_device(): lax.all_gather(key_one, 'sp', axis=0, tiled=True)  57.3 us
    all_to_all x1, waiting for transfers between devices, on_device(): lax.all_to_all(summed, 'sp', split_axis=0, concat_axis=0, tiled=True)  37.2 us
    reduce_scatter x1, waiting for transfers between devices, on_device(): lax.psum_scatter(partial_value.astype(jnp.bfloat16), 'tp', scatter_dimens...  12.6 us
    all_gather x1, waiting for transfers between devices, on_device(): lax.all_gather(lax.all_to_all(outgoing, 'sp', split_axis=0, concat_axis=0...  11.4 us
  transfers between devices with their start and end apart: 6, of which 6 were waited for; matrix products, arithmetic and copies ran while one was open for 2% of the time, Pallas kernels for 0%

commit v1 on v0

v1 whole, which is shorter than its diff:
```python
import functools

import jax
import jax.numpy as jnp
from jax import lax
from jax.experimental import pallas as pl
from jax.experimental.pallas import tpu as pltpu
from jax.sharding import PartitionSpec as P

MESH = pl.DeviceIdType.MESH
EPS = 1e-06
LOW = -1e30
BF = jnp.bfloat16
F32 = jnp.float32
ANY = pl.BlockSpec(memory_space=pl.ANY)
VM = pl.BlockSpec(memory_space=pltpu.VMEM)
DMA = pltpu.SemaphoreType.DMA


def rcopy(src, dst, ssem, rsem, peer):
    return pltpu.make_async_remote_copy(
        src_ref=src, dst_ref=dst, send_sem=ssem, recv_sem=rsem, device_id=peer, device_id_type=MESH
    )


def greet(peers):
    barrier = pltpu.get_barrier_semaphore()
    for peer in peers:
        pl.semaphore_signal(barrier, inc=1, device_id=peer, device_id_type=MESH)
    pl.semaphore_wait(barrier, len(peers))


def pack_kernel(nh, q1, k1, q2, k2, v, q_out, kv_out):
    hd = q1.shape[1] // nh
    vd = v.shape[1] // nh
    scale = hd ** (-0.5)
    for h in range(nh):
        a, b = h * hd, (h + 1) * hd
        q = jnp.concatenate([q1[:, a:b], q2[:, a:b]], axis=1).astype(F32) * scale
        q_out[h] = q.astype(BF)
        kv_out[h, :, : 2 * hd] = jnp.concatenate([k1[:, a:b], k2[:, a:b]], axis=1)
        kv_out[h, :, 2 * hd :] = v[:, h * vd : (h + 1) * vd]


def gather_kernel(
    n, nh, q_ref, kv_ref, g_ref, u_ref, d_ref, q_out, kv_out, g_out, u_out, d_out,
    qs, qr, ks, kr, fs, fr, ws, wr, ls,
):
    np_ = n // nh
    m = np_.bit_length() - 1
    s = lax.axis_index("sp")
    t = lax.axis_index("tp")
    zi = s // np_
    r = s % np_

    def flip(x, bit):
        w = 1 << bit
        return x + w * (1 - 2 * ((x // w) % 2))

    zpeers = [None] + [((zi + d) % nh) for d in range(1, nh)]
    peers = [(zp * np_ + r, t) for zp in zpeers[1:]]
    peers += [(zi * np_ + flip(r, b), t) for b in range(m)]
    peers += [(s, 1 - t)]
    greet(peers)

    own_kv = pltpu.make_async_copy(kv_ref.at[zi], kv_out.at[s], ls.at[0])
    own_q = pltpu.make_async_copy(q_ref.at[zi], q_out.at[zi], ls.at[1])
    own_kv.start()
    own_q.start()
    kcopies, qcopies = [None], []
    for d in range(1, nh):
        zp = zpeers[d]
        c = rcopy(kv_ref.at[zp], kv_out.at[s], ks.at[d], kr.at[d], (zp * np_ + r, t))
        c.start()
        kcopies.append(c)
    for d in range(1, nh):
        zp = zpeers[d]
        c = rcopy(q_ref.at[zp], q_out.at[zi], qs.at[d], qr.at[d], (zp * np_ + r, t))
        c.start()
        qcopies.append(c)
    wcopies = []
    for i, (a, b) in enumerate(((g_ref, g_out), (u_ref, u_out), (d_ref, d_out))):
        c = rcopy(a, b, ws.at[i], wr.at[i], (s, 1 - t))
        c.start()
        wcopies.append(c)
    own_kv.wait()

    def phase(d, p):
        base = ((zi + nh - d) % nh) * np_
        peer = (zi * np_ + flip(r, (p + d) % m), t)
        out = []
        for c in range(1 << p):
            rr = r
            for b in range(p):
                if (c >> b) & 1:
                    rr = flip(rr, (b + d) % m)
            i = d * (np_ - 1) + (1 << p) - 1 + c
            blk = kv_out.at[base + rr]
            e = rcopy(blk, blk, fs.at[i], fr.at[i], peer)
            out.append(e)
        return out

    live = {}
    for d in range(nh):
        if d:
            kcopies[d].wait_recv()
        live[d, 0] = phase(d, 0)
        for e in live[d, 0]:
            e.start()
    for p in range(1, m):
        for d in range(nh):
            for e in live[d, p - 1]:
                e.wait_recv()
            live[d, p] = phase(d, p)
            for e in live[d, p]:
                e.start()
    for d in range(nh):
        for e in live[d, m - 1]:
            e.wait_recv()
        for p in range(m):
            for e in live[d, p]:
                e.wait_send()
    for c in kcopies[1:]:
        c.wait_send()
    for c in qcopies + wcopies:
        c.wait()
    own_q.wait()


def attention_kernel(np_, q_ref, kv_ref, lam_ref, gain_ref, out_ref):
    s = lax.axis_index("sp")
    jq = pl.program_id(0) * np_ + s % np_
    zi = s // np_
    rows, two = q_ref.shape[1], q_ref.shape[2]
    hd = two // 2
    vd = kv_ref.shape[2] - two
    q = q_ref[0]
    lane = lax.broadcasted_iota(jnp.int32, (rows, two), 1)
    zero = jnp.zeros((), BF)
    qs = (jnp.where(lane < hd, q, zero), jnp.where(lane >= hd, q, zero))

    def step(j, state, masked):
        k = kv_ref[j, :, :two]
        v = kv_ref[j, :, two:]
        out = []
        for i in range(2):
            mx, l, acc = state[i]
            sc = lax.dot_general(qs[i], k, (((1,), (1,)), ((), ())), preferred_element_type=F32)
            if masked:
                ri = lax.broadcasted_iota(jnp.int32, sc.shape, 0)
                ci = lax.broadcasted_iota(jnp.int32, sc.shape, 1)
                sc = jnp.where(ri >= ci, sc, LOW)
            new = jnp.maximum(mx, jnp.max(sc, axis=1, keepdims=True))
            p = jnp.exp(sc - new)
            f = jnp.exp(mx - new)
            l = l * f + jnp.sum(p, axis=1, keepdims=True)
            acc = acc * f + jnp.dot(p.astype(BF), v, preferred_element_type=F32)
            out.append((new, l, acc))
        return tuple(out)

    empty = (jnp.full((rows, 1), LOW, F32), jnp.zeros((rows, 1), F32), jnp.zeros((rows, vd), F32))
    state = lax.fori_loop(0, jq, lambda j, st: step(j, st, False), (empty, empty))
    (_, l1, a1), (_, l2, a2) = step(jq, state, True)
    o = a1 / l1 - lam_ref[zi] * (a2 / l2)
    o = o * lax.rsqrt(jnp.mean(o * o, axis=1, keepdims=True) + EPS) * gain_ref[...]
    out_ref[0] = o.astype(BF)


def heads_kernel(n, nt, nh, o_ref, a_ref, ss, rs, ls):
    np_ = n // nh
    s = lax.axis_index("sp")
    t = lax.axis_index("tp")
    zi = s // np_
    r = s % np_
    half = o_ref.shape[1] // nt
    vd = o_ref.shape[2]
    cols = pl.ds(pl.multiple_of((t * nh + zi) * vd, vd), vd)
    combos = [(dz, dt) for dz in range(nh) for dt in range(nt) if dz or dt]
    where = [((zi + dz) % nh, (t + dt) % nt) for dz, dt in combos]
    greet([(z * np_ + r, tp) for z, tp in where])
    own = pltpu.make_async_copy(
        o_ref.at[zi, pl.ds(pl.multiple_of(t * half, half), half)], a_ref.at[:, cols], ls
    )
    own.start()
    copies = []
    for i, (z, tp) in enumerate(where):
        c = rcopy(
            o_ref.at[z, pl.ds(pl.multiple_of(tp * half, half), half)],
            a_ref.at[:, cols], ss.at[i], rs.at[i], (z * np_ + r, tp),
        )
        c.start()
        copies.append(c)
    own.wait()
    for c in copies:
        c.wait()


def route_kernel(ne, cap, capp, a_ref, w_ref, res_ref, gain_ref, ids_ref, after_ref, d0_ref, d1_ref, out_ref):
    rows = a_ref.shape[0]
    proj = jnp.dot(a_ref[...], w_ref[...], preferred_element_type=F32)
    after = (res_ref[...].astype(F32) + proj).astype(BF)
    after_ref[...] = after
    af = after.astype(F32)
    routed = (
        af * lax.rsqrt(jnp.mean(af * af, axis=1, keepdims=True) + EPS) * gain_ref[...]
    ).astype(BF)
    slots = ne * capp
    ids = ids_ref[...]
    ex = lax.broadcasted_iota(jnp.int32, (rows, ne), 1)
    oh0 = (ids[:, 0:1] == ex).astype(F32)
    oh1 = (ids[:, 1:2] == ex).astype(F32)
    tri = (
        lax.broadcasted_iota(jnp.int32, (rows, rows), 0)
        > lax.broadcasted_iota(jnp.int32, (rows, rows), 1)
    ).astype(F32).astype(BF)
    rank = jnp.dot(tri, (oh0 + oh1).astype(BF), preferred_element_type=F32)
    er = lax.broadcasted_iota(jnp.int32, (ne, slots), 0) * capp
    sl = lax.broadcasted_iota(jnp.int32, (ne, slots), 1)
    place = sl - er
    spread = ((place >= 0) & (place < capp)).astype(F32)
    sb = spread.astype(BF)
    slot_in = jnp.sum(jnp.where(spread > 0.0, place.astype(F32), 0.0), axis=0, keepdims=True)
    rank_x = jnp.dot(rank.astype(BF), sb, preferred_element_type=F32)
    hit = jnp.where(rank_x == slot_in, 1.0, 0.0)
    d0 = (jnp.dot(oh0.astype(BF), sb, preferred_element_type=F32) * hit).astype(BF)
    d1 = (jnp.dot(oh1.astype(BF), sb, preferred_element_type=F32) * hit).astype(BF)
    d0_ref[...] = d0
    d1_ref[...] = d1
    out_ref[...] = lax.dot_general(
        d0 + d1, routed, (((0,), (0,)), ((), ())), preferred_element_type=F32
    ).astype(BF)


def swap_kernel(n, x_ref, y_ref, stage, ss, rs, ls):
    s = lax.axis_index("sp")
    t = lax.axis_index("tp")
    greet([((s + d) % n, t) for d in range(1, n)])
    copies = []
    for d in range(1, n):
        p = (s + d) % n
        c = rcopy(x_ref.at[p], y_ref.at[s], ss.at[d], rs.at[d], (p, t))
        c.start()
        copies.append(c)
    a = pltpu.make_async_copy(x_ref.at[s], stage, ls.at[0])
    a.start()
    a.wait()
    b = pltpu.make_async_copy(stage, y_ref.at[s], ls.at[1])
    b.start()
    b.wait()
    for c in copies:
        c.wait()


def swap(x, n, cid):
    return pl.pallas_call(
        functools.partial(swap_kernel, n),
        out_shape=jax.ShapeDtypeStruct(x.shape, x.dtype),
        in_specs=[ANY],
        out_specs=ANY,
        scratch_shapes=[pltpu.VMEM(x.shape[1:], x.dtype), DMA((n,)), DMA((n,)), DMA((2,))],
        compiler_params=pltpu.CompilerParams(collective_id=cid, has_side_effects=True),
        name="swap%d" % cid,
    )(x)


def ffn_kernel(x_ref, g1, u1, d1, g2, u2, d2, y_ref):
    x = x_ref[...]
    total = None
    for g, u, d in ((g1, u1, d1), (g2, u2, d2)):
        gate = jnp.dot(x, g[...], preferred_element_type=F32)
        up = jnp.dot(x, u[...], preferred_element_type=F32)
        hid = (gate * jax.nn.sigmoid(gate) * up).astype(BF)
        part = jnp.dot(hid, d[...], preferred_element_type=F32)
        total = part if total is None else total + part
    y_ref[...] = total.astype(BF)


def combine_kernel(ret_ref, d0_ref, d1_ref, rw_ref, after_ref, out_ref):
    ret = ret_ref[...]
    rw = rw_ref[...]
    a = jnp.dot(d0_ref[...], ret, preferred_element_type=F32) * rw[:, 0:1]
    b = jnp.dot(d1_ref[...], ret, preferred_element_type=F32) * rw[:, 1:2]
    out_ref[...] = (after_ref[...].astype(F32) + (a + b)).astype(BF)


def on_device(
    residual, query_one, key_one, query_two, key_two, value_rows, lambda_head, head_gain,
    out_weight, norm_gain, route_ids, route_weights, gate_weight, up_weight, down_weight,
):
    n = lax.axis_size("sp")
    nt = lax.axis_size("tp")
    nh = lambda_head.shape[0]
    np_ = n // nh
    rows = query_one.shape[0]
    hd = query_one.shape[1] // nh
    vd = value_rows.shape[1] // nh
    wid = residual.shape[1]
    local = residual.shape[0]
    sds = jax.ShapeDtypeStruct

    q, kv = pl.pallas_call(
        functools.partial(pack_kernel, nh),
        out_shape=(sds((nh, rows, 2 * hd), BF), sds((nh, rows, 2 * hd + vd), BF)),
        in_specs=[VM] * 5,
        out_specs=(VM, VM),
        name="pack",
    )(query_one, key_one, query_two, key_two, value_rows)

    g, u, dn = gate_weight[0], up_weight[0], down_weight[0]
    nf = nh * (np_ - 1)
    q_all, kv_all, g2, u2, dn2 = pl.pallas_call(
        functools.partial(gather_kernel, n, nh),
        out_shape=(
            sds((nh, rows, 2 * hd), BF), sds((n, rows, 2 * hd + vd), BF),
            sds(g.shape, BF), sds(u.shape, BF), sds(dn.shape, BF),
        ),
        in_specs=[VM, VM, ANY, ANY, ANY],
        out_specs=(VM, VM, ANY, ANY, ANY),
        scratch_shapes=[
            DMA((nh,)), DMA((nh,)), DMA((nh,)), DMA((nh,)), DMA((nf,)), DMA((nf,)),
            DMA((3,)), DMA((3,)), DMA((2,)),
        ],
        compiler_params=pltpu.CompilerParams(collective_id=1, has_side_effects=True),
        name="gather_heads",
    )(q, kv, g, u, dn)

    attended = pl.pallas_call(
        functools.partial(attention_kernel, np_),
        out_shape=sds((nh, rows, vd), BF),
        grid=(nh,),
        in_specs=[
            pl.BlockSpec((1, rows, 2 * hd), lambda i: (i, 0, 0)),
            VM,
            pl.BlockSpec(memory_space=pltpu.SMEM),
            VM,
        ],
        out_specs=pl.BlockSpec((1, rows, vd), lambda i: (i, 0, 0)),
        name="attend",
    )(q_all, kv_all, lambda_head, head_gain.reshape(1, vd))

    na = nh * nt - 1
    all_heads = pl.pallas_call(
        functools.partial(heads_kernel, n, nt, nh),
        out_shape=sds((rows // nt, nh * nt * vd), BF),
        in_specs=[VM],
        out_specs=VM,
        scratch_shapes=[DMA((na,)), DMA((na,)), DMA],
        compiler_params=pltpu.CompilerParams(collective_id=2, has_side_effects=True),
        name="return_heads",
    )(attended)

    ne = gate_weight.shape[0] * n
    cap = max(2, (3 * rows + 2 * n - 1) // (2 * n))
    capp = (cap + 7) // 8 * 8
    slots = ne * capp
    after, d0, d1, outgoing = pl.pallas_call(
        functools.partial(route_kernel, ne, cap, capp),
        out_shape=(
            sds((local, wid), BF), sds((local, slots), BF), sds((local, slots), BF), sds((slots, wid), BF),
        ),
        in_specs=[VM] * 5,
        out_specs=(VM, VM, VM, VM),
        name="project_route",
    )(all_heads, out_weight, residual, norm_gain.reshape(1, wid), route_ids)

    arrived = swap(outgoing.reshape(ne, capp, wid), n, 3)

    tile = slots // 2
    full = lambda i: (0, 0)
    y = pl.pallas_call(
        ffn_kernel,
        out_shape=sds((slots, wid), BF),
        grid=(2,),
        in_specs=[pl.BlockSpec((tile, wid), lambda i: (i, 0))] + [VM] * 6,
        out_specs=pl.BlockSpec((tile, wid), lambda i: (i, 0)),
        name="ffn",
    )(arrived.reshape(slots, wid), g, u, dn, g2, u2, dn2)

    returned = swap(y.reshape(ne, capp, wid), n, 4)

    return pl.pallas_call(
        combine_kernel,
        out_shape=sds((local, wid), BF),
        in_specs=[VM] * 5,
        out_specs=VM,
        name="combine",
    )(returned.reshape(slots, wid), d0, d1, route_weights, after)


def solution(mesh):
    placed = (
        P(("sp", "tp"), None), P("sp", "tp"), P("sp", "tp"), P("sp", "tp"), P("sp", "tp"),
        P("sp", "tp"), P("tp"), P(), P(), P(), P(("sp", "tp"), None), P(("sp", "tp"), None),
        P("sp", None, "tp"), P("sp", None, "tp"), P("sp", "tp", None),
    )
    return jax.shard_map(
        on_device, mesh=mesh, in_specs=placed, out_specs=P(("sp", "tp"), None), check_vma=False
    )
```

time: 431 us -> 178 us (0.41)
  waiting for transfers between devices: 271 us -> 0 us
  Pallas kernels: 0 us -> 174 us
  blocking collectives: 75.8 us -> 0 us
  local copies, waits for them, and re-layouts: 30.4 us -> 1.48 us
  matrix products: 20.6 us -> 0 us
  between operations: 13.5 us -> 0.06 us
  other arithmetic: 10.3 us -> 0 us
  starting transfers between devices: 7.31 us -> 0 us
    all_gather x4 -> x0, waiting for transfers between devices: 221 us -> none  [the longest x1 86.9 us: on_device(): lax.all_gather(value_rows, 'sp', axis=0, tiled=True)]
    pallas_call x0 -> x9, Pallas kernels: none -> 174 us  [the longest x2 80.7 us: swap(): pl.pallas_call(functools.partial(swap_kernel, n), out_shape=jax.ShapeDtyp...]
    all_to_all x2 -> x0, blocking collectives: 75.8 us -> none  [the longest x1 71.9 us: on_device(): lax.all_to_all(outgoing, 'sp', split_axis=0, concat_axis=0, tiled=True)]
    all_to_all x1 -> x0, waiting for transfers between devices: 37.2 us -> none  [on_device(): lax.all_to_all(summed, 'sp', split_axis=0, concat_axis=0, tiled=True)]
    dot_general x20 -> x0, matrix products: 20.6 us -> none  [the longest x8 5.98 us: online_update(): jnp.einsum('qhk,khd->qhd', exp_weights.astype(jnp.bfloat16), values_block...]
    reduce_scatter x1 -> x0, waiting for transfers between devices: 12.6 us -> none  [on_device(): lax.psum_scatter(partial_value.astype(jnp.bfloat16), 'tp', scatter_dimens...]
    dynamic_slice x12 -> x0, local copies, waits for them, and re-layouts: 12.1 us -> none  [the longest x4 4.33 us: advance(): lax.dynamic_slice_in_dim(pieces[2], begin_row, width_block, 0)]
    reduce_sum x7 -> x0, other arithmetic: 7.61 us -> none  [the longest x4 4.13 us: online_update(): running_sum = running_sum * factor + jnp.sum(exp_weights, axis=-1)]
  transfers between devices with their start and end apart: 6 -> 0, of which waited for: 6 -> 0; matrix products, arithmetic and copies ran while one was open for 2% -> 0% of each run, Pallas kernels for 0% -> 0%
where the time goes in v1:
time: 178 us; the launch traced here: 176 us
  Pallas kernels  174 us (98%)
    pallas_call x2, Pallas kernels, swap(): pl.pallas_call(functools.partial(swap_kernel, n), out_shape=jax.ShapeDtyp...  80.7 us
    pallas_call x1, Pallas kernels, on_device(): pl.pallas_call(functools.partial(gather_kernel, n, nh), out_shape=(sds((n...  35.3 us
    pallas_call x1, Pallas kernels, on_device(): pl.pallas_call(functools.partial(attention_kernel, np_), out_shape=sds((n...  30.7 us
    pallas_call x1, Pallas kernels, on_device(): pl.pallas_call(functools.partial(heads_kernel, n, nt, nh), out_shape=sds(...  10.1 us
    pallas_call x1, Pallas kernels, on_device(): pl.pallas_call(ffn_kernel, out_shape=sds((slots, wid), BF), grid=(2,), in...  6.99 us
    pallas_call x1, Pallas kernels, on_device(): pl.pallas_call(functools.partial(route_kernel, ne, cap, capp), out_shape=...  5.11 us

profile of v1, /device:TPU:12, one launch (start us, length us, event | category | flops | bytes accessed | tf_op | source)
XLA Modules:
  0.0 175.9 jit_solution(2129379172792852466)
XLA Ops:
  0.0 2.3 %pack.1 = (bf16[4,256,128]{2,1,0:T(8,128)(2,1)}, bf16[4,256,256]{2,1,0:T(8,128)(2,1)}) custom-call(bf16[256,256]{1,0:T(8,128)(2,1)} %q1.1, bf16[256,256]{1,0:T(8,128)(2,1)} %k1.1, bf16[256,256]{1,0:T(8,128)(2,1)} %q2.1, bf16[256,256]{1,0:T(8,128)(2,1)} %k2.1, bf16[256,512]{1,0:T(8,128)(2,1)} %v.1), custom_call_target="tpu_custom_call" | custom-call | tf_op jit(solution)/shard_map/pack/pallas_call | solution.py:301
  2.3 35.3 %gather_heads.1 = (bf16[4,256,128]{2,1,0:T(8,128)(2,1)}, bf16[16,256,256]{2,1,0:T(8,128)(2,1)}, bf16[2048,256]{1,0:T(8,128)(2,1)}, bf16[2048,256]{1,0:T(8,128)(2,1)}, bf16[256,2048]{1,0:T(8,128)(2,1)}) custom-call(bf16[4,256,128]{2,1,0:T(8,128)(2,1)} %get-tuple-element.16.q_ref, bf16[4,256,256]{2,1,0:T(8,128)(2,1)} %get-tuple-element.17.kv_ref, ...), custom_call_target="tpu_custom_call" | custom-call | tf_op jit(solution)/shard_map/gather_heads/pallas_call | solution.py:311
  37.6 0.0 copy-start
  37.6 30.7 %attend.1.o_ref = bf16[4,256,128]{2,1,0:T(8,128)(2,1)} custom-call(bf16[4,256,128]{2,1,0:T(8,128)(2,1)} %get-tuple-element.18.q_ref, bf16[16,256,256]{2,1,0:T(8,128)(2,1)} %get-tuple-element.19.kv_ref, f32[4]{0:T(128)} %lam_ref.1, f32[1,128]{1,0:T(1,128)} %bitcast.20), custom_call_target="tpu_custom_call" | custom-call | tf_op jit(solution)/shard_map/attend/pallas_call | solution.py:327
  68.3 10.1 %return_heads.1.a_ref = bf16[128,1024]{1,0:T(8,128)(2,1)} custom-call(bf16[4,256,128]{2,1,0:T(8,128)(2,1)} %attend.1.o_ref), custom_call_target="tpu_custom_call" | custom-call | tf_op jit(solution)/shard_map/return_heads/pallas_call | solution.py:342
  78.4 0.0 copy-done
  78.4 0.7 copy.16.ids_ref
  79.2 5.1 %project_route.1 = (bf16[128,2048]{1,0:T(8,128)(2,1)}, bf16[128,384]{1,0:T(8,128)(2,1)}, bf16[128,384]{1,0:T(8,128)(2,1)}, bf16[384,2048]{1,0:T(8,128)(2,1)}) custom-call(bf16[128,1024]{1,0:T(8,128)(2,1)} %return_heads.1.a_ref, bf16[1024,2048]{1,0:T(8,128)(2,1)} %w_ref.1, bf16[128,2048]{1,0:T(8,128)(2,1)} %res_ref.1, f32[1,2048]{1,0:T(1,128)} %bitcast.19, ...), custom_call_target="tpu_custom_call" | custom-call | tf_op jit(solution)/shard_map/project_route/pallas_call | solution.py:356
  84.3 41.6 %swap3.1 = bf16[16,24,2048]{2,1,0:T(8,128)(2,1)} custom-call(bf16[16,24,2048]{2,1,0:T(8,128)(2,1)} %bitcast.18), custom_call_target="tpu_custom_call" | custom-call | tf_op jit(solution)/shard_map/swap3/pallas_call | solution.py:255
  125.9 7.0 %ffn.1 = bf16[384,2048]{1,0:T(8,128)(2,1)} custom-call(bf16[384,2048]{1,0:T(8,128)(2,1)} %bitcast.9, bf16[2048,256]{1,0:T(8,128)(2,1)} %bitcast.13, bf16[2048,256]{1,0:T(8,128)(2,1)} %bitcast.15, bf16[256,2048]{1,0:T(8,128)(2,1)} %bitcast.17, bf16[2048,256]{1,0:T(8,128)(2,1)} %get-tuple-element.21.g2, bf16[2048,256]{1,0:T(8,128)(2,1)} %get-tuple-element.22.u2, ...), custom_call_target="tpu_custom_call" | custom-call | tf_op jit(solution)/shard_map/ffn/pallas_call | solution.py:370
  132.8 0.0 copy-start.1
  132.8 39.1 %swap4.1 = bf16[16,24,2048]{2,1,0:T(8,128)(2,1)} custom-call(bf16[16,24,2048]{2,1,0:T(8,128)(2,1)} %bitcast.10), custom_call_target="tpu_custom_call" | custom-call | tf_op jit(solution)/shard_map/swap4/pallas_call | solution.py:255
  172.0 0.0 copy-done.1
  172.0 0.7 copy.17.rw_ref
  172.7 3.2 %combine.1 = bf16[128,2048]{1,0:T(8,128)(2,1)} custom-call(bf16[384,2048]{1,0:T(8,128)(2,1)} %bitcast.11, bf16[128,384]{1,0:T(8,128)(2,1)} %get-tuple-element.24.d0_ref, bf16[128,384]{1,0:T(8,128)(2,1)} %get-tuple-element.25.d1_ref, f32[128,2]{1,0:T(8,128)} %copy.17.rw_ref, bf16[128,2048]{1,0:T(8,128)(2,1)} %get-tuple-element.26.after_ref), custom_call_target="tpu_custom_call" | custom-call | tf_op jit(solution)/shard_map/combine/pallas_call | solution.py:381
Async XLA Ops:
  37.6 40.8 %copy-start = (s32[128,2]{0,1:T(2,128)S(1)}, s32[128,2]{0,1:T(2,128)}, u32[]{:S(2)}) copy-start(s32[128,2]{0,1:T(2,128)} %param.25) | copy-start | bytes 3076
  132.8 39.1 %copy-start.1 = (f32[128,2]{0,1:T(2,128)S(1)}, f32[128,2]{0,1:T(2,128)}, u32[]{:S(2)}) copy-start(f32[128,2]{0,1:T(2,128)} %param.26) | copy-start | bytes 3076

commit v2 on v1

--- a/solution.py
+++ b/solution.py
@@ -127,41 +127,64 @@
     own_q.wait()
 
 
-def attention_kernel(np_, q_ref, kv_ref, lam_ref, gain_ref, out_ref):
+def attention_kernel(np_, q_ref, kv_ref, lam_ref, gain_ref, out_ref, s_scr, m_scr, acc_scr):
     s = lax.axis_index("sp")
     jq = pl.program_id(0) * np_ + s % np_
     zi = s // np_
     rows, two = q_ref.shape[1], q_ref.shape[2]
     hd = two // 2
     vd = kv_ref.shape[2] - two
+    group = min(np_, 4)
     q = q_ref[0]
     lane = lax.broadcasted_iota(jnp.int32, (rows, two), 1)
     zero = jnp.zeros((), BF)
-    qs = (jnp.where(lane < hd, q, zero), jnp.where(lane >= hd, q, zero))
-
-    def step(j, state, masked):
-        k = kv_ref[j, :, :two]
-        v = kv_ref[j, :, two:]
-        out = []
-        for i in range(2):
-            mx, l, acc = state[i]
-            sc = lax.dot_general(qs[i], k, (((1,), (1,)), ((), ())), preferred_element_type=F32)
+    qs = jnp.concatenate([jnp.where(lane < hd, q, zero), jnp.where(lane >= hd, q, zero)], axis=0)
+    m_scr[...] = jnp.full(m_scr.shape, LOW, F32)
+    acc_scr[...] = jnp.zeros(acc_scr.shape, F32)
+    lanes = m_scr.shape[1]
+
+    def score(j0, count, masked):
+        best = m_scr[...]
+        for c in range(count):
+            k = kv_ref[j0 + c, :, :two]
+            sc = lax.dot_general(qs, k, (((1,), (1,)), ((), ())), preferred_element_type=F32)
             if masked:
-                ri = lax.broadcasted_iota(jnp.int32, sc.shape, 0)
-                ci = lax.broadcasted_iota(jnp.int32, sc.shape, 1)
-                sc = jnp.where(ri >= ci, sc, LOW)
-            new = jnp.maximum(mx, jnp.max(sc, axis=1, keepdims=True))
-            p = jnp.exp(sc - new)
-            f = jnp.exp(mx - new)
-            l = l * f + jnp.sum(p, axis=1, keepdims=True)
-            acc = acc * f + jnp.dot(p.astype(BF), v, preferred_element_type=F32)
-            out.append((new, l, acc))
-        return tuple(out)
-
-    empty = (jnp.full((rows, 1), LOW, F32), jnp.zeros((rows, 1), F32), jnp.zeros((rows, vd), F32))
-    state = lax.fori_loop(0, jq, lambda j, st: step(j, st, False), (empty, empty))
-    (_, l1, a1), (_, l2, a2) = step(jq, state, True)
-    o = a1 / l1 - lam_ref[zi] * (a2 / l2)
+                ri = lax.broadcasted_iota(jnp.int32, (rows, rows), 0)
+                ci = lax.broadcasted_iota(jnp.int32, (rows, rows), 1)
+                ok = ri >= ci
+                sc = jnp.concatenate(
+                    [jnp.where(ok, sc[:rows], LOW), jnp.where(ok, sc[rows:], LOW)], axis=0
+                )
+            s_scr[j0 + c] = sc
+            for i in range(rows // lanes):
+                best = jnp.maximum(best, sc[:, i * lanes : (i + 1) * lanes])
+        m_scr[...] = best
+
+    def weigh(j0, count):
+        top = m_scr[...]
+        parts = []
+        for c in range(count):
+            sc = s_scr[j0 + c]
+            for i in range(rows // lanes):
+                parts.append(jnp.exp(sc[:, i * lanes : (i + 1) * lanes] - top).astype(BF))
+        p = jnp.concatenate(parts, axis=1)
+        v = kv_ref[pl.ds(j0, count), :, two:].reshape(count * rows, vd)
+        v = jnp.concatenate([v, jnp.ones((count * rows, vd), BF)], axis=1)
+        acc_scr[...] += jnp.dot(p, v, preferred_element_type=F32)
+
+    def loop(lo, hi, fn):
+        lax.fori_loop(lo, hi, lambda j, c: (fn(j), c)[1], 0)
+
+    groups = jq // group
+    loop(0, groups, lambda j: score(j * group, group, False))
+    loop(groups * group, jq, lambda j: score(j, 1, False))
+    score(jq, 1, True)
+    m_scr[...] = jnp.broadcast_to(jnp.max(m_scr[...], axis=1, keepdims=True), m_scr.shape)
+    loop(0, groups, lambda j: weigh(j * group, group))
+    loop(groups * group, jq + 1, lambda j: weigh(j, 1))
+    a1 = acc_scr[:rows, :vd] / acc_scr[:rows, vd:]
+    a2 = acc_scr[rows:, :vd] / acc_scr[rows:, vd:]
+    o = a1 - lam_ref[zi] * a2
     o = o * lax.rsqrt(jnp.mean(o * o, axis=1, keepdims=True) + EPS) * gain_ref[...]
     out_ref[0] = o.astype(BF)
 
@@ -231,56 +254,91 @@
     ).astype(BF)
 
 
-def swap_kernel(n, x_ref, y_ref, stage, ss, rs, ls):
+def moe_kernel(
+    n, nz, x_ref, g1, u1, d1, g2, u2, d2, d0_ref, d1_ref, rw_ref, after_ref, out_ref,
+    arr, ys, ret, gw, uw, dw, ss, rs, bs, br, ls, ws,
+):
+    np_ = n // nz
     s = lax.axis_index("sp")
     t = lax.axis_index("tp")
+    zi = s // np_
+    r = s % np_
+    capp, wid = arr.shape[1], arr.shape[2]
+
+    def plane(mask):
+        z = zi
+        for b in range(nz.bit_length() - 1):
+            if (mask >> b) & 1:
+                w = 1 << b
+                z = z + w * (1 - 2 * ((zi // w) % 2))
+        return z
+
     greet([((s + d) % n, t) for d in range(1, n)])
-    copies = []
-    for d in range(1, n):
-        p = (s + d) % n
-        c = rcopy(x_ref.at[p], y_ref.at[s], ss.at[d], rs.at[d], (p, t))
-        c.start()
-        copies.append(c)
-    a = pltpu.make_async_copy(x_ref.at[s], stage, ls.at[0])
-    a.start()
-    a.wait()
-    b = pltpu.make_async_copy(stage, y_ref.at[s], ls.at[1])
-    b.start()
-    b.wait()
-    for c in copies:
-        c.wait()
-
-
-def swap(x, n, cid):
-    return pl.pallas_call(
-        functools.partial(swap_kernel, n),
-        out_shape=jax.ShapeDtypeStruct(x.shape, x.dtype),
-        in_specs=[ANY],
-        out_specs=ANY,
-        scratch_shapes=[pltpu.VMEM(x.shape[1:], x.dtype), DMA((n,)), DMA((n,)), DMA((2,))],
-        compiler_params=pltpu.CompilerParams(collective_id=cid, has_side_effects=True),
-        name="swap%d" % cid,
-    )(x)
-
-
-def ffn_kernel(x_ref, g1, u1, d1, g2, u2, d2, y_ref):
-    x = x_ref[...]
-    total = None
-    for g, u, d in ((g1, u1, d1), (g2, u2, d2)):
-        gate = jnp.dot(x, g[...], preferred_element_type=F32)
-        up = jnp.dot(x, u[...], preferred_element_type=F32)
-        hid = (gate * jax.nn.sigmoid(gate) * up).astype(BF)
-        part = jnp.dot(hid, d[...], preferred_element_type=F32)
-        total = part if total is None else total + part
-    y_ref[...] = total.astype(BF)
-
-
-def combine_kernel(ret_ref, d0_ref, d1_ref, rw_ref, after_ref, out_ref):
-    ret = ret_ref[...]
+    masks = list(range(nz - 1, -1, -1))
+    sends, backs, selfs = {}, {}, []
+    for w in masks:
+        sends[w] = []
+        for c in range(np_):
+            if w == 0 and c == 0:
+                e = pltpu.make_async_copy(x_ref.at[s], arr.at[s], ls.at[0])
+                e.start()
+                selfs.append(e)
+                continue
+            p = plane(w) * np_ + (r + c) % np_
+            i = w * np_ + c
+            e = rcopy(x_ref.at[p], arr.at[s], ss.at[i], rs.at[i], (p, t))
+            e.start()
+            sends[w].append(e)
+    loads = []
+    for i, (a, b) in enumerate(
+        ((g1, gw.at[0]), (g2, gw.at[1]), (u1, uw.at[0]), (u2, uw.at[1]), (d1, dw.at[0]), (d2, dw.at[1]))
+    ):
+        e = pltpu.make_async_copy(a, b, ws.at[i])
+        e.start()
+        loads.append(e)
+    for e in loads:
+        e.wait()
+
+    order = [nz - 1, 0] + list(range(1, nz - 1))
+    for w in order:
+        for e in sends[w]:
+            e.wait_recv()
+        if w == 0:
+            selfs[0].wait()
+        base = plane(w) * np_
+        x = arr[pl.ds(base, np_)].astype(F32).reshape(np_ * capp, wid).astype(BF)
+        total = None
+        for i in range(2):
+            gate = jnp.dot(x, gw[i], preferred_element_type=F32)
+            up = jnp.dot(x, uw[i], preferred_element_type=F32)
+            hid = (gate * jax.nn.sigmoid(gate) * up).astype(BF)
+            part = jnp.dot(hid, dw[i], preferred_element_type=F32)
+            total = part if total is None else total + part
+        ys[pl.ds(base, np_)] = total.reshape(np_, capp, wid).astype(BF)
+        backs[w] = []
+        for c in range(np_):
+            if w == 0 and c == 0:
+                e = pltpu.make_async_copy(ys.at[s], ret.at[s], ls.at[1])
+                e.start()
+                selfs.append(e)
+                continue
+            p = base + (r + c) % np_
+            i = w * np_ + c
+            e = rcopy(ys.at[p], ret.at[s], bs.at[i], br.at[i], (p, t))
+            e.start()
+            backs[w].append(e)
+    for w in order:
+        for e in backs[w]:
+            e.wait_recv()
+    selfs[1].wait()
+    back = ret[...].astype(F32).reshape(n * capp, wid).astype(BF)
     rw = rw_ref[...]
-    a = jnp.dot(d0_ref[...], ret, preferred_element_type=F32) * rw[:, 0:1]
-    b = jnp.dot(d1_ref[...], ret, preferred_element_type=F32) * rw[:, 1:2]
+    a = jnp.dot(d0_ref[...], back, preferred_element_type=F32) * rw[:, 0:1]
+    b = jnp.dot(d1_ref[...], back, preferred_element_type=F32) * rw[:, 1:2]
     out_ref[...] = (after_ref[...].astype(F32) + (a + b)).astype(BF)
+    for w in order:
+        for e in sends[w] + backs[w]:
+            e.wait_send()
 
 
 def on_device(
@@ -335,6 +393,11 @@
             VM,
         ],
         out_specs=pl.BlockSpec((1, rows, vd), lambda i: (i, 0, 0)),
+        scratch_shapes=[
+            pltpu.VMEM((n, 2 * rows, rows), F32),
+            pltpu.VMEM((2 * rows, min(rows, 128)), F32),
+            pltpu.VMEM((2 * rows, 2 * vd), F32),
+        ],
         name="attend",
     )(q_all, kv_all, lambda_head, head_gain.reshape(1, vd))
 
@@ -363,28 +426,21 @@
         name="project_route",
     )(all_heads, out_weight, residual, norm_gain.reshape(1, wid), route_ids)
 
-    arrived = swap(outgoing.reshape(ne, capp, wid), n, 3)
-
-    tile = slots // 2
-    full = lambda i: (0, 0)
-    y = pl.pallas_call(
-        ffn_kernel,
-        out_shape=sds((slots, wid), BF),
-        grid=(2,),
-        in_specs=[pl.BlockSpec((tile, wid), lambda i: (i, 0))] + [VM] * 6,
-        out_specs=pl.BlockSpec((tile, wid), lambda i: (i, 0)),
-        name="ffn",
-    )(arrived.reshape(slots, wid), g, u, dn, g2, u2, dn2)
-
-    returned = swap(y.reshape(ne, capp, wid), n, 4)
-
+    ff = g.shape[1]
+    block = (n, capp, wid)
     return pl.pallas_call(
-        combine_kernel,
+        functools.partial(moe_kernel, n, nh),
         out_shape=sds((local, wid), BF),
-        in_specs=[VM] * 5,
+        in_specs=[ANY] * 7 + [VM] * 4,
         out_specs=VM,
-        name="combine",
-    )(returned.reshape(slots, wid), d0, d1, route_weights, after)
+        scratch_shapes=[
+            pltpu.VMEM(block, BF), pltpu.VMEM(block, BF), pltpu.VMEM(block, BF),
+            pltpu.VMEM((2, wid, ff), BF), pltpu.VMEM((2, wid, ff), BF), pltpu.VMEM((2, ff, wid), BF),
+            DMA((n,)), DMA((n,)), DMA((n,)), DMA((n,)), DMA((2,)), DMA((6,)),
+        ],
+        compiler_params=pltpu.CompilerParams(collective_id=3, has_side_effects=True),
+        name="experts",
+    )(outgoing.reshape(block), g, u, dn, g2, u2, dn2, d0, d1, route_weights, after)
 
 
 def solution(mesh):

time: 178 us -> 151 us (0.85)
  the two profiles are of different devices: /device:TPU:12 before, /device:TPU:0 now
where the time goes in v2:
time: 151 us
  Pallas kernels  148 us (98%)
  local copies, waits for them, and re-layouts  3.37 us (2%)
    pallas_call x1, Pallas kernels, on_device(): pl.pallas_call(functools.partial(moe_kernel, n, nh), out_shape=sds((local...  81.9 us
    pallas_call x1, Pallas kernels, on_device(): pl.pallas_call(functools.partial(gather_kernel, n, nh), out_shape=(sds((n...  33.1 us
    pallas_call x1, Pallas kernels, on_device(): pl.pallas_call(functools.partial(heads_kernel, n, nt, nh), out_shape=sds(...  14.3 us
    pallas_call x1, Pallas kernels, on_device(): pl.pallas_call(functools.partial(attention_kernel, np_), out_shape=sds((n...  10.8 us
    pallas_call x1, Pallas kernels, on_device(): pl.pallas_call(functools.partial(route_kernel, ne, cap, capp), out_shape=...  5.12 us
    unnamed x7, local copies, waits for them, and re-layouts  3.37 us

profile of v2, /device:TPU:0, one launch (start us, length us, event | category | flops | bytes accessed | tf_op | source)
XLA Modules:
  0.0 150.9 jit_solution(4281922925247110649)
XLA Ops:
  0.0 2.3 %pack.1 = (bf16[4,256,128]{2,1,0:T(8,128)(2,1)}, bf16[4,256,256]{2,1,0:T(8,128)(2,1)}) custom-call(bf16[256,256]{1,0:T(8,128)(2,1)} %q1.1, bf16[256,256]{1,0:T(8,128)(2,1)} %k1.1, bf16[256,256]{1,0:T(8,128)(2,1)} %q2.1, bf16[256,256]{1,0:T(8,128)(2,1)} %k2.1, bf16[256,512]{1,0:T(8,128)(2,1)} %v.1), custom_call_target="tpu_custom_call" | custom-call | tf_op jit(solution)/shard_map/pack/pallas_call | solution.py:359
  2.3 33.1 %gather_heads.1 = (bf16[4,256,128]{2,1,0:T(8,128)(2,1)}, bf16[16,256,256]{2,1,0:T(8,128)(2,1)}, bf16[2048,256]{1,0:T(8,128)(2,1)}, bf16[2048,256]{1,0:T(8,128)(2,1)}, bf16[256,2048]{1,0:T(8,128)(2,1)}) custom-call(bf16[4,256,128]{2,1,0:T(8,128)(2,1)} %get-tuple-element.16.q_ref, bf16[4,256,256]{2,1,0:T(8,128)(2,1)} %get-tuple-element.17.kv_ref, ...), custom_call_target="tpu_custom_call" | custom-call | tf_op jit(solution)/shard_map/gather_heads/pallas_call | solution.py:369
  35.4 0.0 copy-start
  35.4 10.8 %attend.1.o_ref = bf16[4,256,128]{2,1,0:T(8,128)(2,1)} custom-call(bf16[4,256,128]{2,1,0:T(8,128)(2,1)} %get-tuple-element.18.q_ref, bf16[16,256,256]{2,1,0:T(8,128)(2,1)} %get-tuple-element.19.kv_ref, f32[4]{0:T(128)} %lam_ref.1, f32[1,128]{1,0:T(1,128)} %bitcast.14), custom_call_target="tpu_custom_call" | custom-call | tf_op jit(solution)/shard_map/attend/pallas_call | solution.py:385
  46.2 14.3 %return_heads.1.a_ref = bf16[128,1024]{1,0:T(8,128)(2,1)} custom-call(bf16[4,256,128]{2,1,0:T(8,128)(2,1)} %attend.1.o_ref), custom_call_target="tpu_custom_call" | custom-call | tf_op jit(solution)/shard_map/return_heads/pallas_call | solution.py:405
  60.5 0.0 copy-done
  60.6 0.7 copy.16.ids_ref
  61.3 0.0 copy-start.1
  61.3 5.1 %project_route.1 = (bf16[128,2048]{1,0:T(8,128)(2,1)}, bf16[128,384]{1,0:T(8,128)(2,1)}, bf16[128,384]{1,0:T(8,128)(2,1)}, bf16[384,2048]{1,0:T(8,128)(2,1)}) custom-call(bf16[128,1024]{1,0:T(8,128)(2,1)} %return_heads.1.a_ref, bf16[1024,2048]{1,0:T(8,128)(2,1)} %w_ref.1, bf16[128,2048]{1,0:T(8,128)(2,1)} %res_ref.1, f32[1,2048]{1,0:T(1,128)} %bitcast.13, ...), custom_call_target="tpu_custom_call" | custom-call | tf_op jit(solution)/shard_map/project_route/pallas_call | solution.py:419
  66.4 0.0 copy-done.1
  66.4 0.7 copy.17.rw_ref
  67.2 81.9 %experts.1 = bf16[128,2048]{1,0:T(8,128)(2,1)} custom-call(bf16[16,24,2048]{2,1,0:T(8,128)(2,1)} %bitcast.12, bf16[2048,256]{1,0:T(8,128)(2,1)} %bitcast.7, bf16[2048,256]{1,0:T(8,128)(2,1)} %bitcast.9, bf16[256,2048]{1,0:T(8,128)(2,1)} %bitcast.11, bf16[2048,256]{1,0:T(8,128)(2,1)} %get-tuple-element.21.g2, bf16[2048,256]{1,0:T(8,128)(2,1)} %get-tuple-element.22.u2, ...), custom_call_target="tpu_custom_call" | custom-call | tf_op jit(solution)/shard_map/experts/pallas_call | solution.py:431
  149.0 1.9 %copy.19 = bf16[128,2048]{1,0:T(8,128)(2,1)} copy(bf16[128,2048]{1,0:T(8,128)(2,1)} %experts.1) | data formatting | bytes 1048576
Async XLA Ops:
  35.4 25.1 %copy-start = (s32[128,2]{0,1:T(2,128)S(1)}, s32[128,2]{0,1:T(2,128)}, u32[]{:S(2)}) copy-start(s32[128,2]{0,1:T(2,128)} %param.25) | copy-start | bytes 3076
  61.3 5.1 %copy-start.1 = (f32[128,2]{0,1:T(2,128)S(1)}, f32[128,2]{0,1:T(2,128)}, u32[]{:S(2)}) copy-start(f32[128,2]{0,1:T(2,128)} %param.26) | copy-start | bytes 3076
